TPU v7x, 128 devices: a whole 4x4x4 slice. The times are simulated.
128 devices in a mesh: sp: 64 (over z, y, x), tp: 2 (over core).
Axes of the slice: x: 4, y: 4, z: 4, core: 2. Of those that a mesh axis runs over, the one named last changes fastest.
Arguments:
- stream: bfloat16 [16384, 2048], P(('sp', 'tp')), may hold values from -3 to 3
- query_narrow: bfloat16 [16384, 1024], P('sp', 'tp'), may hold values from -6 to 6
- key_narrow: bfloat16 [16384, 128], P('sp', 'tp'), may hold values from -6 to 6
- value_narrow: bfloat16 [16384, 128], P('sp', 'tp'), may hold values from -6 to 6
- query_broad: bfloat16 [16384, 1024], P('sp', 'tp'), may hold values from -6 to 6
- key_broad: bfloat16 [16384, 256], P('sp', 'tp'), may hold values from -6 to 6
- value_broad: bfloat16 [16384, 256], P('sp', 'tp'), may hold values from -6 to 6
- narrow_query_gain: float32 [64], replicated, may hold values from 1.5 to 9
- narrow_key_gain: float32 [64], replicated, may hold values from 1.5 to 9
- broad_query_gain: float32 [128], replicated, may hold values from 1.5 to 9
- broad_key_gain: float32 [128], replicated, may hold values from 1.5 to 9
- out_weight: bfloat16 [2048, 2048], replicated, may hold values from -0.125 to 0.125
- norm_gain: float32 [2048], replicated, may hold values from 0.1 to 1.9
- gate_weight: bfloat16 [64, 2048, 1024], P('sp', None, 'tp'), may hold values from -0.125 to 0.125
- up_weight: bfloat16 [64, 2048, 1024], P('sp', None, 'tp'), may hold values from -0.125 to 0.125
- down_weight: bfloat16 [64, 1024, 2048], P('sp', 'tp'), may hold values from -0.1875 to 0.1875
- route_ids: int32 [16384, 2], P(('sp', 'tp')), may hold values from 0 to 63, all different within a row; in each aligned block of 128 rows (0 to 127, 128 to 255, ...) at most 8 rows name the same one
- route_weights: float32 [16384, 2], P(('sp', 'tp')), may hold values from 0.1 to 1
Outputs:
- result: bfloat16 [16384, 2048], P(('sp', 'tp'))
Inputs may be any that keep to these rules, and one draw needn't show every extreme that they name: `route_ids`: in each aligned block of 128 rows no expert is named by more than 8 rows, a bound that some block reaches.
All inputs are finite; a program needn't handle non-finite values.
Results may differ from a plain program's by a relative error of at most 0.015.
The roundings to bfloat16 on the way count: a program that leaves them out, or rounds other values in their place, can miss the bound.
Values may be sent and summed in bfloat16 or wider, within the bound.
A program may use at most 128 MiB of HBM per device.

v0:
```python
import math
import jax
import jax.numpy as jnp
from jax import lax
from jax.sharding import PartitionSpec as P

HA = 16
DA = 64
DB = 128
GRID_W = 128
eps = 1e-06
theta = 10000.0


def cut_along(value, dim, size):
    before, after = (value.shape[:dim], value.shape[dim + 1 :])
    return jnp.moveaxis(value.reshape(*before, size, -1, *after), dim, 0)


def summed_on_arrival(value, axis, dim):
    size = lax.axis_size(axis)
    blocks = lax.all_to_all(cut_along(value, dim, size), axis, 0, 0, tiled=True)
    return jnp.sum(blocks.astype(jnp.float32), axis=0)


def joined_along(blocks, dim):
    shape = list(blocks.shape[1:])
    shape[dim] *= blocks.shape[0]
    return jnp.moveaxis(blocks, 0, dim).reshape(shape)


def copy_for_each(value, axis):
    size = lax.axis_size(axis)
    return lax.all_to_all(
        jnp.broadcast_to(value[None], (size, *value.shape)), axis, 0, 0, tiled=True
    )


def gather_directly(value, axis, dim):
    return joined_along(copy_for_each(value, axis), dim)


def rotate_grid(normed, positions):
    count, heads, dim = normed.shape
    freqs = dim // 4
    inverse = theta ** (-jnp.arange(freqs, dtype=jnp.float32) / freqs)
    rows = (positions // GRID_W).astype(jnp.float32)
    cols = (positions % GRID_W).astype(jnp.float32)
    angles = jnp.stack([rows[:, None] * inverse, cols[:, None] * inverse], axis=1)
    cosine = jnp.cos(angles)[:, None]
    sine = jnp.sin(angles)[:, None]
    split = normed.reshape(count, heads, 2, 2, freqs)
    first = split[..., 0, :]
    second = split[..., 1, :]
    turned = jnp.stack([first * cosine - second * sine, second * cosine + first * sine], axis=-2)
    return turned.reshape(count, heads, dim)


def prepare(raw, gain, dim, positions):
    count = raw.shape[0]
    values = raw.astype(jnp.float32).reshape(count, -1, dim)
    scaled = values * lax.rsqrt(jnp.mean(values * values, axis=-1, keepdims=True) + eps) * gain
    return rotate_grid(scaled, positions).reshape(count, -1).astype(jnp.bfloat16)


def arrange(queries, kv_width, dim):
    rows = queries.shape[0]
    heads_kv = kv_width // dim
    shaped = queries.reshape(rows, heads_kv, -1, dim)
    groups = shaped.shape[2]
    start = (
        jnp.full((heads_kv, groups, rows), -1e30, jnp.float32),
        jnp.zeros((heads_kv, groups, rows), jnp.float32),
        jnp.zeros((heads_kv, groups, rows, dim), jnp.float32),
    )
    return (shaped, start)


def attend_block(state, queries, keys, values):
    peak, total, summed = state
    dim = queries.shape[-1]
    scores = jnp.einsum(
        "qhgd,khd->hgqk", queries, keys, preferred_element_type=jnp.float32
    ) * dim ** (-0.5)
    fresh = jnp.maximum(peak, jnp.max(scores, axis=-1))
    weights = jnp.exp(scores - fresh[..., None])
    shrink = jnp.exp(peak - fresh)
    total = total * shrink + jnp.sum(weights, axis=-1)
    summed = summed * shrink[..., None] + jnp.einsum(
        "hgqk,khd->hgqd", weights.astype(jnp.bfloat16), values, preferred_element_type=jnp.float32
    )
    return (fresh, total, summed)


def sweep(state, keys, values, queries):
    rows = keys.shape[0]
    size = math.gcd(rows, 2048)
    count = rows // size

    def step(carry, block):
        return (attend_block(carry, queries, block[0], block[1]), None)

    blocks = (
        keys.reshape(count, size, keys.shape[1], keys.shape[2]),
        values.reshape(count, size, values.shape[1], values.shape[2]),
    )
    state, _ = lax.scan(step, state, blocks)
    return state


def make_fold(shaped_n, shaped_b, state, pieces):
    keys_n, values_n, keys_b, values_b = pieces
    rows = keys_n.shape[0]
    first = sweep(state[0], keys_n.reshape(rows, -1, DA), values_n.reshape(rows, -1, DA), shaped_n)
    second = sweep(state[1], keys_b.reshape(rows, -1, DB), values_b.reshape(rows, -1, DB), shaped_b)
    return (first, second)


def finish(state):
    peak, total, summed = state
    heads_out = summed / total[..., None]
    rows = heads_out.shape[2]
    return jnp.transpose(heads_out, (2, 0, 1, 3)).reshape(rows, -1).astype(jnp.bfloat16)


def local(
    stream,
    query_narrow,
    key_narrow,
    value_narrow,
    query_broad,
    key_broad,
    value_broad,
    narrow_query_gain,
    narrow_key_gain,
    broad_query_gain,
    broad_key_gain,
    out_weight,
    norm_gain,
    gate_weight,
    up_weight,
    down_weight,
    route_ids,
    route_weights,
):
    count = query_narrow.shape[0]
    positions = lax.axis_index("sp") * count + jnp.arange(count, dtype=jnp.int32)
    queries_n = prepare(query_narrow, narrow_query_gain, DA, positions)
    keys_n = prepare(key_narrow, narrow_key_gain, DA, positions)
    queries_b = prepare(query_broad, broad_query_gain, DB, positions)
    keys_b = prepare(key_broad, broad_key_gain, DB, positions)
    shaped_n, start_n = arrange(queries_n, keys_n.shape[1], DA)
    shaped_b, start_b = arrange(queries_b, keys_b.shape[1], DB)
    state = make_fold(
        shaped_n,
        shaped_b,
        (start_n, start_b),
        (
            lax.all_gather(keys_n, "sp", axis=0, tiled=True),
            lax.all_gather(value_narrow, "sp", axis=0, tiled=True),
            lax.all_gather(keys_b, "sp", axis=0, tiled=True),
            lax.all_gather(value_broad, "sp", axis=0, tiled=True),
        ),
    )
    heads_n = finish(state[0])
    heads_b = finish(state[1])
    width = heads_n.shape[1]
    place = lax.axis_index("tp")
    local_weight = jnp.concatenate(
        [
            lax.dynamic_slice_in_dim(out_weight, place * width, width, 0),
            lax.dynamic_slice_in_dim(out_weight, HA * DA + place * width, width, 0),
        ],
        axis=0,
    )
    local_heads = jnp.concatenate([heads_n, heads_b], axis=1)
    picked = local_heads
    mixed = summed_on_arrival(
        jnp.dot(picked, local_weight, preferred_element_type=jnp.float32).astype(jnp.bfloat16),
        "tp",
        0,
    )
    wide = (stream.astype(jnp.float32) + mixed).astype(jnp.bfloat16).astype(jnp.float32)
    normed = (
        wide * lax.rsqrt(jnp.mean(wide * wide, axis=-1, keepdims=True) + eps) * norm_gain
    ).astype(jnp.bfloat16)
    tokens_here, topk = route_ids.shape
    width_model = normed.shape[1]
    experts = lax.axis_size("sp")
    capacity = (2 * tokens_here * topk + experts - 1) // experts
    flat = route_ids.reshape(-1)
    hits = (flat[:, None] == jnp.arange(experts, dtype=jnp.int32)[None, :]).astype(jnp.int32)
    ranks = jnp.sum((jnp.cumsum(hits, axis=0) - 1) * hits, axis=1)
    slots = flat * capacity + ranks
    table = (jnp.arange(experts * capacity, dtype=jnp.int32)[:, None] == slots[None, :]).astype(
        jnp.bfloat16
    )
    table = jnp.sum(table.reshape(experts * capacity, tokens_here, topk), axis=2)
    sent = jnp.dot(table, normed, preferred_element_type=jnp.float32).astype(jnp.bfloat16)
    sent = sent.reshape(experts, capacity, width_model)
    piece = gather_directly(
        lax.all_to_all(sent, "sp", split_axis=0, concat_axis=0, tiled=True), "tp", 0
    )
    rows = piece.reshape(-1, piece.shape[-1])
    gate = jnp.dot(rows, gate_weight[0], preferred_element_type=jnp.float32)
    upper = jnp.dot(rows, up_weight[0], preferred_element_type=jnp.float32)
    hidden = (jax.nn.silu(gate) * upper).astype(jnp.bfloat16)
    partial_out = jnp.dot(hidden, down_weight[0], preferred_element_type=jnp.float32).astype(
        jnp.bfloat16
    )
    terms = lax.optimization_barrier(partial_out).astype(jnp.float32).reshape(piece.shape)
    summed = summed_on_arrival(terms.astype(jnp.bfloat16), "tp", 0).astype(jnp.bfloat16)
    back = lax.all_to_all(summed, "sp", split_axis=0, concat_axis=0, tiled=True)
    picked = jnp.take(back.reshape(experts * capacity, width_model), slots, axis=0)
    picked = picked.astype(jnp.float32).reshape(tokens_here, topk, width_model)
    routed = jnp.sum(picked * route_weights[..., None], axis=1)
    return (wide + routed).astype(jnp.bfloat16)


def solution(mesh):
    return jax.shard_map(
        local,
        mesh=mesh,
        in_specs=(
            P(("sp", "tp"), None),
            P("sp", "tp"),
            P("sp", "tp"),
            P("sp", "tp"),
            P("sp", "tp"),
            P("sp", "tp"),
            P("sp", "tp"),
            P(),
            P(),
            P(),
            P(),
            P(),
            P(),
            P("sp", None, "tp"),
            P("sp", None, "tp"),
            P("sp", "tp", None),
            P(("sp", "tp"), None),
            P(("sp", "tp"), None),
        ),
        out_specs=P(("sp", "tp"), None),
        check_vma=False,
    )
```

profile of v0, /device:TPU:0, one launch (start us, length us, event | category | flops | bytes accessed | tf_op | source)
XLA Modules:
  0.0 630.0 jit_solution(12985772197260481180)
XLA Ops:
  25.9 53.0 %all-gather.5.cloned.1.call-done = bf16[16384,64]{0,1:T(8,128)(2,1)} async-done(((bf16[256,64]{0,1:T(8,128)(2,1)}), bf16[16384,64]{0,1:T(8,128)(2,1)}) %all-gather.5.cloned.1.call-update) | async-done | bytes 2097168 | tf_op jit(solution)/shard_map/all_gather | solution.py:159
  84.2 63.0 %all-gather.7.cloned.1.call-done = bf16[16384,64]{0,1:T(8,128)(2,1)} async-done(((bf16[256,64]{0,1:T(8,128)(2,1)}), bf16[16384,64]{0,1:T(8,128)(2,1)}) %all-gather.7.cloned.1.call-update) | async-done | bytes 2097168 | tf_op jit(solution)/shard_map/all_gather | solution.py:160
  152.5 219.9 %while.30 = (s32[]{:T(128)}, f32[1,8,256]{2,1,0:T(8,128)S(1)}, f32[1,8,256]{2,1,0:T(8,128)S(1)}, f32[1,8,256,64]{2,3,1,0:T(8,128)}, bf16[8,2048,1,64]{1,3,2,0:T(...) while((s32[]{:T(128)}, f32[1,8,256]{2,1,0:T(8,128)S(1)}, ...), condition=%wide.region_5.6_spmd.clone, body=%wide.region_2.5_spmd.clone.sunk | while | flops 1107701760 | bytes 52298852 | solution.py:107
  152.8 9.0 %bitcast_reduce_fusion.6 = (f32[8,256]{1,0:T(8,128)S(1)}, f32[2048,256,8]{1,0,2:T(8,128)}) fusion(bf16[256,1,8,64]{0,3,2,1:T(8,128)(2,1)S(1)} %get-tuple-element.395, bf16[8,2048,1,64]{1,3,2,0:T(8,128)(2,1)} %get-tuple-element.394, s32[]{:T(128)} %get-tuple-element.381), kind=kOutput, calls=%fused_computation.2.clone.1 | convolution fusion | flops 545257472 | bytes 17310208 | tf_op jit(solution)/shard_map/while/body/eval_jaxpr/qhgd,khd->hgqk/dot_general | solution.py:82
  161.8 9.6 %fusion.116 = f32[1,8,256,64]{2,3,1,0:T(8,128)} fusion(f32[2048,256,8]{1,0,2:T(8,128)} %get-tuple-element.332, f32[8,256]{1,0:T(8,128)S(1)} %bitcast.237, f32[1,8,256,64]{2,3,1,0:T(8,128)} %get-tuple-element.384, bf16[8,2048,1,64]{1,3,2,0:T(8,128)(2,1)} %get-tuple-element.396, s32[]{:T(128)} %get-tuple-element.381, ...), kind=kOutput, calls=%fused_computation.9.clone.1 | convolution fusion | flops 549847040 | bytes 18104832 | tf_op jit(solution)/shard_map/while/body/eval_jaxpr/hgqk,khd->hgqd/dot_general | solution.py:89
  180.1 9.0 %bitcast_reduce_fusion.6 = (f32[8,256]{1,0:T(8,128)S(1)}, f32[2048,256,8]{1,0,2:T(8,128)}) fusion(bf16[256,1,8,64]{0,3,2,1:T(8,128)(2,1)S(1)} %get-tuple-element.395, bf16[8,2048,1,64]{1,3,2,0:T(8,128)(2,1)} %get-tuple-element.394, s32[]{:T(128)} %get-tuple-element.381), kind=kOutput, calls=%fused_computation.2.clone.1 | convolution fusion | flops 545257472 | bytes 17310208 | tf_op jit(solution)/shard_map/while/body/eval_jaxpr/qhgd,khd->hgqk/dot_general | solution.py:82
  189.1 9.7 %fusion.116 = f32[1,8,256,64]{2,3,1,0:T(8,128)} fusion(f32[2048,256,8]{1,0,2:T(8,128)} %get-tuple-element.332, f32[8,256]{1,0:T(8,128)S(1)} %bitcast.237, f32[1,8,256,64]{2,3,1,0:T(8,128)} %get-tuple-element.384, bf16[8,2048,1,64]{1,3,2,0:T(8,128)(2,1)} %get-tuple-element.396, s32[]{:T(128)} %get-tuple-element.381, ...), kind=kOutput, calls=%fused_computation.9.clone.1 | convolution fusion | flops 549847040 | bytes 18104832 | tf_op jit(solution)/shard_map/while/body/eval_jaxpr/hgqk,khd->hgqd/dot_general | solution.py:89
  207.8 9.0 %bitcast_reduce_fusion.6 = (f32[8,256]{1,0:T(8,128)S(1)}, f32[2048,256,8]{1,0,2:T(8,128)}) fusion(bf16[256,1,8,64]{0,3,2,1:T(8,128)(2,1)S(1)} %get-tuple-element.395, bf16[8,2048,1,64]{1,3,2,0:T(8,128)(2,1)} %get-tuple-element.394, s32[]{:T(128)} %get-tuple-element.381), kind=kOutput, calls=%fused_computation.2.clone.1 | convolution fusion | flops 545257472 | bytes 17310208 | tf_op jit(solution)/shard_map/while/body/eval_jaxpr/qhgd,khd->hgqk/dot_general | solution.py:82
  216.8 10.0 %fusion.116 = f32[1,8,256,64]{2,3,1,0:T(8,128)} fusion(f32[2048,256,8]{1,0,2:T(8,128)} %get-tuple-element.332, f32[8,256]{1,0:T(8,128)S(1)} %bitcast.237, f32[1,8,256,64]{2,3,1,0:T(8,128)} %get-tuple-element.384, bf16[8,2048,1,64]{1,3,2,0:T(8,128)(2,1)} %get-tuple-element.396, s32[]{:T(128)} %get-tuple-element.381, ...), kind=kOutput, calls=%fused_computation.9.clone.1 | convolution fusion | flops 549847040 | bytes 18104832 | tf_op jit(solution)/shard_map/while/body/eval_jaxpr/hgqk,khd->hgqd/dot_general | solution.py:89
  235.4 9.0 %bitcast_reduce_fusion.6 = (f32[8,256]{1,0:T(8,128)S(1)}, f32[2048,256,8]{1,0,2:T(8,128)}) fusion(bf16[256,1,8,64]{0,3,2,1:T(8,128)(2,1)S(1)} %get-tuple-element.395, bf16[8,2048,1,64]{1,3,2,0:T(8,128)(2,1)} %get-tuple-element.394, s32[]{:T(128)} %get-tuple-element.381), kind=kOutput, calls=%fused_computation.2.clone.1 | convolution fusion | flops 545257472 | bytes 17310208 | tf_op jit(solution)/shard_map/while/body/eval_jaxpr/qhgd,khd->hgqk/dot_general | solution.py:82
  244.5 9.7 %fusion.116 = f32[1,8,256,64]{2,3,1,0:T(8,128)} fusion(f32[2048,256,8]{1,0,2:T(8,128)} %get-tuple-element.332, f32[8,256]{1,0:T(8,128)S(1)} %bitcast.237, f32[1,8,256,64]{2,3,1,0:T(8,128)} %get-tuple-element.384, bf16[8,2048,1,64]{1,3,2,0:T(8,128)(2,1)} %get-tuple-element.396, s32[]{:T(128)} %get-tuple-element.381, ...), kind=kOutput, calls=%fused_computation.9.clone.1 | convolution fusion | flops 549847040 | bytes 18104832 | tf_op jit(solution)/shard_map/while/body/eval_jaxpr/hgqk,khd->hgqd/dot_general | solution.py:89
  262.8 9.1 %bitcast_reduce_fusion.6 = (f32[8,256]{1,0:T(8,128)S(1)}, f32[2048,256,8]{1,0,2:T(8,128)}) fusion(bf16[256,1,8,64]{0,3,2,1:T(8,128)(2,1)S(1)} %get-tuple-element.395, bf16[8,2048,1,64]{1,3,2,0:T(8,128)(2,1)} %get-tuple-element.394, s32[]{:T(128)} %get-tuple-element.381), kind=kOutput, calls=%fused_computation.2.clone.1 | convolution fusion | flops 545257472 | bytes 17310208 | tf_op jit(solution)/shard_map/while/body/eval_jaxpr/qhgd,khd->hgqk/dot_general | solution.py:82
  271.9 9.7 %fusion.116 = f32[1,8,256,64]{2,3,1,0:T(8,128)} fusion(f32[2048,256,8]{1,0,2:T(8,128)} %get-tuple-element.332, f32[8,256]{1,0:T(8,128)S(1)} %bitcast.237, f32[1,8,256,64]{2,3,1,0:T(8,128)} %get-tuple-element.384, bf16[8,2048,1,64]{1,3,2,0:T(8,128)(2,1)} %get-tuple-element.396, s32[]{:T(128)} %get-tuple-element.381, ...), kind=kOutput, calls=%fused_computation.9.clone.1 | convolution fusion | flops 549847040 | bytes 18104832 | tf_op jit(solution)/shard_map/while/body/eval_jaxpr/hgqk,khd->hgqd/dot_general | solution.py:89
  290.5 9.0 %bitcast_reduce_fusion.6 = (f32[8,256]{1,0:T(8,128)S(1)}, f32[2048,256,8]{1,0,2:T(8,128)}) fusion(bf16[256,1,8,64]{0,3,2,1:T(8,128)(2,1)S(1)} %get-tuple-element.395, bf16[8,2048,1,64]{1,3,2,0:T(8,128)(2,1)} %get-tuple-element.394, s32[]{:T(128)} %get-tuple-element.381), kind=kOutput, calls=%fused_computation.2.clone.1 | convolution fusion | flops 545257472 | bytes 17310208 | tf_op jit(solution)/shard_map/while/body/eval_jaxpr/qhgd,khd->hgqk/dot_general | solution.py:82
  299.6 9.7 %fusion.116 = f32[1,8,256,64]{2,3,1,0:T(8,128)} fusion(f32[2048,256,8]{1,0,2:T(8,128)} %get-tuple-element.332, f32[8,256]{1,0:T(8,128)S(1)} %bitcast.237, f32[1,8,256,64]{2,3,1,0:T(8,128)} %get-tuple-element.384, bf16[8,2048,1,64]{1,3,2,0:T(8,128)(2,1)} %get-tuple-element.396, s32[]{:T(128)} %get-tuple-element.381, ...), kind=kOutput, calls=%fused_computation.9.clone.1 | convolution fusion | flops 549847040 | bytes 18104832 | tf_op jit(solution)/shard_map/while/body/eval_jaxpr/hgqk,khd->hgqd/dot_general | solution.py:89
  317.8 9.0 %bitcast_reduce_fusion.6 = (f32[8,256]{1,0:T(8,128)S(1)}, f32[2048,256,8]{1,0,2:T(8,128)}) fusion(bf16[256,1,8,64]{0,3,2,1:T(8,128)(2,1)S(1)} %get-tuple-element.395, bf16[8,2048,1,64]{1,3,2,0:T(8,128)(2,1)} %get-tuple-element.394, s32[]{:T(128)} %get-tuple-element.381), kind=kOutput, calls=%fused_computation.2.clone.1 | convolution fusion | flops 545257472 | bytes 17310208 | tf_op jit(solution)/shard_map/while/body/eval_jaxpr/qhgd,khd->hgqk/dot_general | solution.py:82
  326.9 9.7 %fusion.116 = f32[1,8,256,64]{2,3,1,0:T(8,128)} fusion(f32[2048,256,8]{1,0,2:T(8,128)} %get-tuple-element.332, f32[8,256]{1,0:T(8,128)S(1)} %bitcast.237, f32[1,8,256,64]{2,3,1,0:T(8,128)} %get-tuple-element.384, bf16[8,2048,1,64]{1,3,2,0:T(8,128)(2,1)} %get-tuple-element.396, s32[]{:T(128)} %get-tuple-element.381, ...), kind=kOutput, calls=%fused_computation.9.clone.1 | convolution fusion | flops 549847040 | bytes 18104832 | tf_op jit(solution)/shard_map/while/body/eval_jaxpr/hgqk,khd->hgqd/dot_general | solution.py:89
  345.1 9.0 %bitcast_reduce_fusion.6 = (f32[8,256]{1,0:T(8,128)S(1)}, f32[2048,256,8]{1,0,2:T(8,128)}) fusion(bf16[256,1,8,64]{0,3,2,1:T(8,128)(2,1)S(1)} %get-tuple-element.395, bf16[8,2048,1,64]{1,3,2,0:T(8,128)(2,1)} %get-tuple-element.394, s32[]{:T(128)} %get-tuple-element.381), kind=kOutput, calls=%fused_computation.2.clone.1 | convolution fusion | flops 545257472 | bytes 17310208 | tf_op jit(solution)/shard_map/while/body/eval_jaxpr/qhgd,khd->hgqk/dot_general | solution.py:82
  354.2 9.7 %fusion.116 = f32[1,8,256,64]{2,3,1,0:T(8,128)} fusion(f32[2048,256,8]{1,0,2:T(8,128)} %get-tuple-element.332, f32[8,256]{1,0:T(8,128)S(1)} %bitcast.237, f32[1,8,256,64]{2,3,1,0:T(8,128)} %get-tuple-element.384, bf16[8,2048,1,64]{1,3,2,0:T(8,128)(2,1)} %get-tuple-element.396, s32[]{:T(128)} %get-tuple-element.381, ...), kind=kOutput, calls=%fused_computation.9.clone.1 | convolution fusion | flops 549847040 | bytes 18104832 | tf_op jit(solution)/shard_map/while/body/eval_jaxpr/hgqk,khd->hgqd/dot_general | solution.py:89
  380.6 103.4 %while.31 = (s32[]{:T(128)}, f32[1,4,256]{2,1,0:T(4,128)S(1)}, f32[1,4,256]{2,1,0:T(4,128)S(1)}, f32[1,4,256,128]{3,2,1,0:T(8,128)S(1)}, bf16[8,2048,1,128]{3,1,...) while((s32[]{:T(128)}, f32[1,4,256]{2,1,0:T(4,128)S(1)}, ...), condition=%wide.region_11.12_spmd.clone, body=%wide.region_8.11_spmd.clone.sunk | while | flops 1090918400 | bytes 61146240 | solution.py:107
  493.8 38.3 %all_to_all.26 = bf16[64,8,2048]{2,1,0:T(8,128)(2,1)S(1)} all-to-all(bf16[64,8,2048]{2,1,0:T(8,128)(2,1)S(1)} %fusion.48), channel_id=1, replica_groups=mesh['sp'=64,'tp'=2] {'sp'}, dimensions={0} | all-to-all | bytes 4194304 | tf_op jit(solution)/shard_map/all_to_all | solution.py:202
  545.8 10.0 %convolution_convert_fusion = bf16[1024,2048]{1,0:T(8,128)(2,1)} fusion(bf16[1,512,2048]{2,1,0:T(8,128)(2,1)S(1)} %copy-done, f32[1024,512]{1,0:T(8,128)} %fusion.53, bf16[1024,2048]{1,0:T(8,128)(2,1)} %bitcast.240, bf16[1,2048,512]{2,1,0:T(8,128)(2,1)} %param.35), kind=kOutput, calls=%fused_computation.53 | convolution fusion | flops 4300210176 | bytes 14680064 | tf_op jit(solution)/shard_map/dot_general | solution.py:208
  555.8 11.9 %all_to_all.28 = bf16[2,64,8,2048]{3,2,1,0:T(8,128)(2,1)} all-to-all(bf16[2,64,8,2048]{3,2,1,0:T(8,128)(2,1)} %bitcast.241), channel_id=1, replica_groups=mesh['sp'=64,'tp'=2] {'tp'}, dimensions={0} | all-to-all | bytes 8388608 | tf_op jit(solution)/shard_map/all_to_all | solution.py:22
  579.5 29.6 %all-to-all-done.4 = bf16[64,8,2048]{2,1,0:T(8,128)(2,1)} async-done(((bf16[64,8,2048]{2,1,0:T(8,128)(2,1)}), bf16[64,8,2048]{2,1,0:T(8,128)(2,1)}, u32[]{:S(2)}, u32[]{:S(2)}) %all-to-all-start.4) | async-done | bytes 2097184 | tf_op jit(solution)/shard_map/all_to_all | solution.py:213
  (211 shorter events, 259.1 us)
Async XLA Ops:
  6.5 539.2 %copy-start = (bf16[1,512,2048]{2,1,0:T(8,128)(2,1)S(1)}, bf16[1,512,2048]{2,1,0:T(8,128)(2,1)}, u32[]{:S(2)}) copy-start(bf16[1,512,2048]{2,1,0:T(8,128)(2,1)} %param.37) | copy-start | bytes 6291460
  6.5 13.6 %copy-start.6 = (s32[128,2]{0,1:T(2,128)S(1)}, s32[128,2]{0,1:T(2,128)}, u32[]{:S(2)}) copy-start(s32[128,2]{0,1:T(2,128)} %param.38) | copy-start | bytes 3076
  6.5 72.4 %all-gather.5.cloned.1.call-start = ((), (), s32[]{:S(2)}) async-start(), calls=%async_computation.5 | async-start | bytes 2129920 | tf_op jit(solution)/shard_map/all_gather | solution.py:159
  9.2 138.0 %all-gather.7.cloned.1.call-start = ((), (), s32[]{:S(2)}) async-start(), calls=%async_computation.6 | async-start | bytes 2129920 | tf_op jit(solution)/shard_map/all_gather | solution.py:160
  9.9 364.3 %all-gather.9.cloned.1.call-start = ((), (), s32[]{:S(2)}) async-start(), calls=%async_computation.7 | async-start | bytes 4259840 | tf_op jit(solution)/shard_map/all_gather | solution.py:161
  12.7 367.8 %all-gather.11.cloned.1.call-start = ((), (), s32[]{:S(2)}) async-start(), calls=%async_computation.8 | async-start | bytes 4259840 | tf_op jit(solution)/shard_map/all_gather | solution.py:162
  19.9 0.8 copy-start.4
  386.6 5.9 copy-start.1
  399.5 5.9 copy-start.1
  412.3 5.9 copy-start.1
  425.2 5.9 copy-start.1
  438.1 5.9 copy-start.1
  450.9 5.9 copy-start.1
  463.8 5.9 copy-start.1
  476.7 5.9 copy-start.1
  487.8 4.9 copy-start.3
  487.8 5.2 copy-start.8
  532.7 9.4 %copy-start.11 = (bf16[1,2048,512]{2,1,0:T(8,128)(2,1)S(1)}, bf16[1,2048,512]{2,1,0:T(8,128)(2,1)}, u32[]{:S(2)}) copy-start(bf16[1,2048,512]{2,1,0:T(8,128)(2,1)} %param.36) | copy-start | bytes 6291460
  540.1 2.0 copy-start.2
  567.7 11.3 %copy-start.7 = (s32[128,2]{0,1:T(2,128)S(1)}, s32[128,2]{0,1:T(2,128)}, u32[]{:S(2)}) copy-start(s32[128,2]{0,1:T(2,128)} %param.38) | copy-start | bytes 3076
  567.7 11.5 %copy-start.9 = (pred[128,2]{0,1:T(4,128)(4,1)S(1)}, pred[128,2]{0,1:T(4,128)(4,1)}, u32[]{:S(2)}) copy-start(pred[128,2]{0,1:T(4,128)(4,1)} %get-tuple-element.207) | copy-start | bytes 772
  567.7 11.7 %copy-start.10 = (f32[128,2]{0,1:T(2,128)S(1)}, f32[128,2]{0,1:T(2,128)}, u32[]{:S(2)}) copy-start(f32[128,2]{0,1:T(2,128)} %param.39) | copy-start | bytes 3076
  567.7 11.8 %copy-start.5 = (s32[256]{0:T(256)S(1)}, s32[256]{0:T(256)}, u32[]{:S(2)}) copy-start(s32[256]{0:T(256)} %copy-done.4) | copy-start | bytes 3076
  572.7 36.4 %all-to-all-start.4 = ((bf16[64,8,2048]{2,1,0:T(8,128)(2,1)}), bf16[64,8,2048]{2,1,0:T(8,128)(2,1)}, u32[]{:S(2)}, u32[]{:S(2)}) async-start(bf16[64,8,2048]{2,1,0:T(8,128)(2,1)} %reduce_sum.131), calls=%async_computation.4 | async-start | bytes 4194304 | tf_op jit(solution)/shard_map/all_to_all | solution.py:213
Sparse Core Ops, SparseCore 0:
  10.0 68.8 all-gather.4
  81.6 65.5 all-gather.6
  149.9 73.9 all-gather.8
  226.7 69.3 all-gather.10
where the time goes:
time: 638 us; the launch traced here: 630 us
  matrix products  254 us (40%)
  waiting for transfers between devices  147 us (23%)
  other arithmetic  101 us (16%)
  blocking collectives  62.3 us (10%)
  local copies, waits for them, and re-layouts  44.2 us (7%)
  between operations  13.7 us (2%)
    dot_general x16, matrix products, attend_block(): jnp.einsum('hgqk,khd->hgqd', weights.astype(jnp.bfloat16), values, prefer...  120 us
    dot_general x16, matrix products, attend_block(): jnp.einsum('qhgd,khd->hgqk', queries, keys, preferred_element_type=jnp.fl...  116 us
    reduce_sum x16, other arithmetic, attend_block(): total = total * shrink + jnp.sum(weights, axis=-1)  80.2 us
    all_gather x1, waiting for transfers between devices, local(): lax.all_gather(value_narrow, 'sp', axis=0, tiled=True)  63 us
    all_gather x1, waiting for transfers between devices, local(): lax.all_gather(keys_n, 'sp', axis=0, tiled=True)  53 us
    all_to_all x1, blocking collectives, local(): lax.all_to_all(sent, 'sp', split_axis=0, concat_axis=0, tiled=True)  38.3 us
    all_to_all x1, waiting for transfers between devices, local(): back = lax.all_to_all(summed, 'sp', split_axis=0, concat_axis=0, tiled=True)  29.6 us
    unnamed x33, local copies, waits for them, and re-layouts  23.1 us
  transfers between devices with their start and end apart: 5, of which 3 were waited for; matrix products, arithmetic and copies ran while one was open for 40% of the time, Pallas kernels for 0%

commit v1 on v0

--- a/solution.py
+++ b/solution.py
@@ -157,7 +157,9 @@
         (start_n, start_b),
         (
             lax.all_gather(keys_n, "sp", axis=0, tiled=True),
-            lax.all_gather(value_narrow, "sp", axis=0, tiled=True),
+            jnp.concatenate(
+                lax.all_to_all(jnp.stack([value_narrow] * lax.axis_size("sp")), "sp", 0, 0), axis=0
+            ),
             lax.all_gather(keys_b, "sp", axis=0, tiled=True),
             lax.all_gather(value_broad, "sp", axis=0, tiled=True),
         ),

time: 638 us -> 588 us (0.922)
  waiting for transfers between devices: 147 us -> 72.3 us
  starting transfers between devices: 6.3 us -> 18.1 us
  local copies, waits for them, and re-layouts: 44.2 us -> 51.8 us
    all_gather x1 -> x0, waiting for transfers between devices: 63 us -> none  [local(): lax.all_gather(value_narrow, 'sp', axis=0, tiled=True)]
    all_gather x1, waiting for transfers between devices: 53 us -> 26.2 us  [local(): lax.all_gather(keys_n, 'sp', axis=0, tiled=True)]
    all_to_all x0 -> x1, waiting for transfers between devices: none -> 15.7 us  [local(): lax.all_to_all(jnp.stack([value_narrow] * lax.axis_size('sp')), 'sp', 0, 0)]
    all_to_all x0 -> x1, starting transfers between devices: none -> 11.8 us  [local(): lax.all_to_all(jnp.stack([value_narrow] * lax.axis_size('sp')), 'sp', 0, 0)]
    another operation x1 -> x3, local copies, waits for them, and re-layouts: 0.02 us -> 6.56 us  [the longest x1 4.21 us: sweep(): values.reshape(count, size, values.shape[1], values.shape[2])]
    unnamed x33 -> x38, local copies, waits for them, and re-layouts: 23.1 us -> 20.3 us
  transfers between devices with their start and end apart: 5 -> 5, of which waited for: 3 -> 3; matrix products, arithmetic and copies ran while one was open for 40% -> 46% of each run, Pallas kernels for 0% -> 0%
where the time goes in v1:
time: 588 us; the launch traced here: 579 us
  matrix products  254 us (43%)
  other arithmetic  105 us (18%)
  waiting for transfers between devices  72.3 us (12%)
  blocking collectives  62.3 us (11%)
  local copies, waits for them, and re-layouts  51.8 us (9%)
  starting transfers between devices  18.1 us (3%)
  between operations  13.8 us (2%)
    dot_general x16, matrix products, attend_block(): jnp.einsum('hgqk,khd->hgqd', weights.astype(jnp.bfloat16), values, prefer...  120 us
    dot_general x16, matrix products, attend_block(): jnp.einsum('qhgd,khd->hgqk', queries, keys, preferred_element_type=jnp.fl...  116 us
    reduce_sum x16, other arithmetic, attend_block(): total = total * shrink + jnp.sum(weights, axis=-1)  80.2 us
    all_to_all x1, blocking collectives, local(): lax.all_to_all(sent, 'sp', split_axis=0, concat_axis=0, tiled=True)  38.3 us
    all_to_all x1, waiting for transfers between devices, local(): back = lax.all_to_all(summed, 'sp', split_axis=0, concat_axis=0, tiled=True)  29.6 us
    all_gather x1, waiting for transfers between devices, local(): lax.all_gather(keys_n, 'sp', axis=0, tiled=True)  26.2 us
    unnamed x38, local copies, waits for them, and re-layouts  20.3 us
    all_to_all x2, blocking collectives, summed_on_arrival(): blocks = lax.all_to_all(cut_along(value, dim, size), axis, 0, 0, tiled=True)  16.6 us
  transfers between devices with their start and end apart: 5, of which 3 were waited for; matrix products, arithmetic and copies ran while one was open for 46% of the time, Pallas kernels for 0%

profile of v1, /device:TPU:0, one launch (start us, length us, event | category | flops | bytes accessed | tf_op | source)
XLA Modules:
  0.0 578.9 jit_solution(17764624282338560809)
XLA Ops:
  15.6 11.8 %all-to-all-start = ((bf16[64,256,64]{1,2,0:T(8,128)(2,1)}), bf16[64,256,64]{1,2,0:T(8,128)(2,1)}, u32[]{:S(2)}, u32[]{:S(2)}) async-start(bf16[64,256,64]{1,2,0:T(8,128)(2,1)} %stack.36), calls=%async_computation | async-start | bytes 4194304 | tf_op jit(solution)/shard_map/all_to_all | solution.py:161
  41.7 15.7 %all-to-all-done = bf16[64,256,64]{1,2,0:T(8,128)(2,1)} async-done(((bf16[64,256,64]{1,2,0:T(8,128)(2,1)}), bf16[64,256,64]{1,2,0:T(8,128)(2,1)}, u32[]{:S(2)}, u32[]{:S(2)}) %all-to-all-start) | async-done | bytes 2097184 | tf_op jit(solution)/shard_map/all_to_all | solution.py:161
  69.9 26.2 %all-gather.4.cloned.1.call-done = bf16[16384,64]{0,1:T(8,128)(2,1)} async-done(((bf16[256,64]{0,1:T(8,128)(2,1)}), bf16[16384,64]{0,1:T(8,128)(2,1)}) %all-gather.4.cloned.1.call-update) | async-done | bytes 2097168 | tf_op jit(solution)/shard_map/all_gather | solution.py:159
  101.3 219.9 %while.30 = (s32[]{:T(128)}, f32[1,8,256]{2,1,0:T(8,128)S(1)}, f32[1,8,256]{2,1,0:T(8,128)S(1)}, f32[1,8,256,64]{2,3,1,0:T(8,128)}, bf16[8,2048,1,64]{1,3,2,0:T(...) while((s32[]{:T(128)}, f32[1,8,256]{2,1,0:T(8,128)S(1)}, ...), condition=%wide.region_5.6_spmd.clone, body=%wide.region_2.5_spmd.clone.sunk | while | flops 1107701760 | bytes 52298852 | solution.py:107
  101.6 9.0 %bitcast_reduce_fusion.6 = (f32[8,256]{1,0:T(8,128)S(1)}, f32[2048,256,8]{1,0,2:T(8,128)}) fusion(bf16[256,1,8,64]{0,3,2,1:T(8,128)(2,1)S(1)} %get-tuple-element.409, bf16[8,2048,1,64]{1,3,2,0:T(8,128)(2,1)} %get-tuple-element.408, s32[]{:T(128)} %get-tuple-element.395), kind=kOutput, calls=%fused_computation.2.clone.1 | convolution fusion | flops 545257472 | bytes 17310208 | tf_op jit(solution)/shard_map/while/body/eval_jaxpr/qhgd,khd->hgqk/dot_general | solution.py:82
  110.6 9.6 %fusion.116 = f32[1,8,256,64]{2,3,1,0:T(8,128)} fusion(f32[2048,256,8]{1,0,2:T(8,128)} %get-tuple-element.346, f32[8,256]{1,0:T(8,128)S(1)} %bitcast.233, f32[1,8,256,64]{2,3,1,0:T(8,128)} %get-tuple-element.398, bf16[8,2048,1,64]{1,3,2,0:T(8,128)(2,1)} %get-tuple-element.410, s32[]{:T(128)} %get-tuple-element.395, ...), kind=kOutput, calls=%fused_computation.9.clone.1 | convolution fusion | flops 549847040 | bytes 18104832 | tf_op jit(solution)/shard_map/while/body/eval_jaxpr/hgqk,khd->hgqd/dot_general | solution.py:89
  128.9 9.0 %bitcast_reduce_fusion.6 = (f32[8,256]{1,0:T(8,128)S(1)}, f32[2048,256,8]{1,0,2:T(8,128)}) fusion(bf16[256,1,8,64]{0,3,2,1:T(8,128)(2,1)S(1)} %get-tuple-element.409, bf16[8,2048,1,64]{1,3,2,0:T(8,128)(2,1)} %get-tuple-element.408, s32[]{:T(128)} %get-tuple-element.395), kind=kOutput, calls=%fused_computation.2.clone.1 | convolution fusion | flops 545257472 | bytes 17310208 | tf_op jit(solution)/shard_map/while/body/eval_jaxpr/qhgd,khd->hgqk/dot_general | solution.py:82
  137.9 9.7 %fusion.116 = f32[1,8,256,64]{2,3,1,0:T(8,128)} fusion(f32[2048,256,8]{1,0,2:T(8,128)} %get-tuple-element.346, f32[8,256]{1,0:T(8,128)S(1)} %bitcast.233, f32[1,8,256,64]{2,3,1,0:T(8,128)} %get-tuple-element.398, bf16[8,2048,1,64]{1,3,2,0:T(8,128)(2,1)} %get-tuple-element.410, s32[]{:T(128)} %get-tuple-element.395, ...), kind=kOutput, calls=%fused_computation.9.clone.1 | convolution fusion | flops 549847040 | bytes 18104832 | tf_op jit(solution)/shard_map/while/body/eval_jaxpr/hgqk,khd->hgqd/dot_general | solution.py:89
  156.6 9.0 %bitcast_reduce_fusion.6 = (f32[8,256]{1,0:T(8,128)S(1)}, f32[2048,256,8]{1,0,2:T(8,128)}) fusion(bf16[256,1,8,64]{0,3,2,1:T(8,128)(2,1)S(1)} %get-tuple-element.409, bf16[8,2048,1,64]{1,3,2,0:T(8,128)(2,1)} %get-tuple-element.408, s32[]{:T(128)} %get-tuple-element.395), kind=kOutput, calls=%fused_computation.2.clone.1 | convolution fusion | flops 545257472 | bytes 17310208 | tf_op jit(solution)/shard_map/while/body/eval_jaxpr/qhgd,khd->hgqk/dot_general | solution.py:82
  165.6 10.0 %fusion.116 = f32[1,8,256,64]{2,3,1,0:T(8,128)} fusion(f32[2048,256,8]{1,0,2:T(8,128)} %get-tuple-element.346, f32[8,256]{1,0:T(8,128)S(1)} %bitcast.233, f32[1,8,256,64]{2,3,1,0:T(8,128)} %get-tuple-element.398, bf16[8,2048,1,64]{1,3,2,0:T(8,128)(2,1)} %get-tuple-element.410, s32[]{:T(128)} %get-tuple-element.395, ...), kind=kOutput, calls=%fused_computation.9.clone.1 | convolution fusion | flops 549847040 | bytes 18104832 | tf_op jit(solution)/shard_map/while/body/eval_jaxpr/hgqk,khd->hgqd/dot_general | solution.py:89
  184.2 9.0 %bitcast_reduce_fusion.6 = (f32[8,256]{1,0:T(8,128)S(1)}, f32[2048,256,8]{1,0,2:T(8,128)}) fusion(bf16[256,1,8,64]{0,3,2,1:T(8,128)(2,1)S(1)} %get-tuple-element.409, bf16[8,2048,1,64]{1,3,2,0:T(8,128)(2,1)} %get-tuple-element.408, s32[]{:T(128)} %get-tuple-element.395), kind=kOutput, calls=%fused_computation.2.clone.1 | convolution fusion | flops 545257472 | bytes 17310208 | tf_op jit(solution)/shard_map/while/body/eval_jaxpr/qhgd,khd->hgqk/dot_general | solution.py:82
  193.3 9.7 %fusion.116 = f32[1,8,256,64]{2,3,1,0:T(8,128)} fusion(f32[2048,256,8]{1,0,2:T(8,128)} %get-tuple-element.346, f32[8,256]{1,0:T(8,128)S(1)} %bitcast.233, f32[1,8,256,64]{2,3,1,0:T(8,128)} %get-tuple-element.398, bf16[8,2048,1,64]{1,3,2,0:T(8,128)(2,1)} %get-tuple-element.410, s32[]{:T(128)} %get-tuple-element.395, ...), kind=kOutput, calls=%fused_computation.9.clone.1 | convolution fusion | flops 549847040 | bytes 18104832 | tf_op jit(solution)/shard_map/while/body/eval_jaxpr/hgqk,khd->hgqd/dot_general | solution.py:89
  211.6 9.1 %bitcast_reduce_fusion.6 = (f32[8,256]{1,0:T(8,128)S(1)}, f32[2048,256,8]{1,0,2:T(8,128)}) fusion(bf16[256,1,8,64]{0,3,2,1:T(8,128)(2,1)S(1)} %get-tuple-element.409, bf16[8,2048,1,64]{1,3,2,0:T(8,128)(2,1)} %get-tuple-element.408, s32[]{:T(128)} %get-tuple-element.395), kind=kOutput, calls=%fused_computation.2.clone.1 | convolution fusion | flops 545257472 | bytes 17310208 | tf_op jit(solution)/shard_map/while/body/eval_jaxpr/qhgd,khd->hgqk/dot_general | solution.py:82
  220.7 9.7 %fusion.116 = f32[1,8,256,64]{2,3,1,0:T(8,128)} fusion(f32[2048,256,8]{1,0,2:T(8,128)} %get-tuple-element.346, f32[8,256]{1,0:T(8,128)S(1)} %bitcast.233, f32[1,8,256,64]{2,3,1,0:T(8,128)} %get-tuple-element.398, bf16[8,2048,1,64]{1,3,2,0:T(8,128)(2,1)} %get-tuple-element.410, s32[]{:T(128)} %get-tuple-element.395, ...), kind=kOutput, calls=%fused_computation.9.clone.1 | convolution fusion | flops 549847040 | bytes 18104832 | tf_op jit(solution)/shard_map/while/body/eval_jaxpr/hgqk,khd->hgqd/dot_general | solution.py:89
  239.3 9.0 %bitcast_reduce_fusion.6 = (f32[8,256]{1,0:T(8,128)S(1)}, f32[2048,256,8]{1,0,2:T(8,128)}) fusion(bf16[256,1,8,64]{0,3,2,1:T(8,128)(2,1)S(1)} %get-tuple-element.409, bf16[8,2048,1,64]{1,3,2,0:T(8,128)(2,1)} %get-tuple-element.408, s32[]{:T(128)} %get-tuple-element.395), kind=kOutput, calls=%fused_computation.2.clone.1 | convolution fusion | flops 545257472 | bytes 17310208 | tf_op jit(solution)/shard_map/while/body/eval_jaxpr/qhgd,khd->hgqk/dot_general | solution.py:82
  248.4 9.7 %fusion.116 = f32[1,8,256,64]{2,3,1,0:T(8,128)} fusion(f32[2048,256,8]{1,0,2:T(8,128)} %get-tuple-element.346, f32[8,256]{1,0:T(8,128)S(1)} %bitcast.233, f32[1,8,256,64]{2,3,1,0:T(8,128)} %get-tuple-element.398, bf16[8,2048,1,64]{1,3,2,0:T(8,128)(2,1)} %get-tuple-element.410, s32[]{:T(128)} %get-tuple-element.395, ...), kind=kOutput, calls=%fused_computation.9.clone.1 | convolution fusion | flops 549847040 | bytes 18104832 | tf_op jit(solution)/shard_map/while/body/eval_jaxpr/hgqk,khd->hgqd/dot_general | solution.py:89
  266.6 9.0 %bitcast_reduce_fusion.6 = (f32[8,256]{1,0:T(8,128)S(1)}, f32[2048,256,8]{1,0,2:T(8,128)}) fusion(bf16[256,1,8,64]{0,3,2,1:T(8,128)(2,1)S(1)} %get-tuple-element.409, bf16[8,2048,1,64]{1,3,2,0:T(8,128)(2,1)} %get-tuple-element.408, s32[]{:T(128)} %get-tuple-element.395), kind=kOutput, calls=%fused_computation.2.clone.1 | convolution fusion | flops 545257472 | bytes 17310208 | tf_op jit(solution)/shard_map/while/body/eval_jaxpr/qhgd,khd->hgqk/dot_general | solution.py:82
  275.7 9.7 %fusion.116 = f32[1,8,256,64]{2,3,1,0:T(8,128)} fusion(f32[2048,256,8]{1,0,2:T(8,128)} %get-tuple-element.346, f32[8,256]{1,0:T(8,128)S(1)} %bitcast.233, f32[1,8,256,64]{2,3,1,0:T(8,128)} %get-tuple-element.398, bf16[8,2048,1,64]{1,3,2,0:T(8,128)(2,1)} %get-tuple-element.410, s32[]{:T(128)} %get-tuple-element.395, ...), kind=kOutput, calls=%fused_computation.9.clone.1 | convolution fusion | flops 549847040 | bytes 18104832 | tf_op jit(solution)/shard_map/while/body/eval_jaxpr/hgqk,khd->hgqd/dot_general | solution.py:89
  303.0 9.7 %fusion.116 = f32[1,8,256,64]{2,3,1,0:T(8,128)} fusion(f32[2048,256,8]{1,0,2:T(8,128)} %get-tuple-element.346, f32[8,256]{1,0:T(8,128)S(1)} %bitcast.233, f32[1,8,256,64]{2,3,1,0:T(8,128)} %get-tuple-element.398, bf16[8,2048,1,64]{1,3,2,0:T(8,128)(2,1)} %get-tuple-element.410, s32[]{:T(128)} %get-tuple-element.395, ...), kind=kOutput, calls=%fused_computation.9.clone.1 | convolution fusion | flops 549847040 | bytes 18104832 | tf_op jit(solution)/shard_map/while/body/eval_jaxpr/hgqk,khd->hgqd/dot_general | solution.py:89
  329.4 103.4 %while.31 = (s32[]{:T(128)}, f32[1,4,256]{2,1,0:T(4,128)S(1)}, f32[1,4,256]{2,1,0:T(4,128)S(1)}, f32[1,4,256,128]{3,2,1,0:T(8,128)S(1)}, bf16[8,2048,1,128]{3,1,...) while((s32[]{:T(128)}, f32[1,4,256]{2,1,0:T(4,128)S(1)}, ...), condition=%wide.region_11.12_spmd.clone, body=%wide.region_8.11_spmd.clone.sunk | while | flops 1090918400 | bytes 61146240 | solution.py:107
  442.6 38.3 %all_to_all.31 = bf16[64,8,2048]{2,1,0:T(8,128)(2,1)S(1)} all-to-all(bf16[64,8,2048]{2,1,0:T(8,128)(2,1)S(1)} %fusion.48), channel_id=1, replica_groups=mesh['sp'=64,'tp'=2] {'sp'}, dimensions={0} | all-to-all | bytes 4194304 | tf_op jit(solution)/shard_map/all_to_all | solution.py:204
  494.6 10.0 %convolution_convert_fusion = bf16[1024,2048]{1,0:T(8,128)(2,1)} fusion(bf16[1,512,2048]{2,1,0:T(8,128)(2,1)S(1)} %copy-done, f32[1024,512]{1,0:T(8,128)} %fusion.53, bf16[1024,2048]{1,0:T(8,128)(2,1)} %bitcast.236, bf16[1,2048,512]{2,1,0:T(8,128)(2,1)} %param.35), kind=kOutput, calls=%fused_computation.53 | convolution fusion | flops 4300210176 | bytes 14680064 | tf_op jit(solution)/shard_map/dot_general | solution.py:210
  504.6 11.9 %all_to_all.33 = bf16[2,64,8,2048]{3,2,1,0:T(8,128)(2,1)} all-to-all(bf16[2,64,8,2048]{3,2,1,0:T(8,128)(2,1)} %bitcast.237), channel_id=1, replica_groups=mesh['sp'=64,'tp'=2] {'tp'}, dimensions={0} | all-to-all | bytes 8388608 | tf_op jit(solution)/shard_map/all_to_all | solution.py:22
  528.3 29.6 %all-to-all-done.5 = bf16[64,8,2048]{2,1,0:T(8,128)(2,1)} async-done(((bf16[64,8,2048]{2,1,0:T(8,128)(2,1)}), bf16[64,8,2048]{2,1,0:T(8,128)(2,1)}, u32[]{:S(2)}, u32[]{:S(2)}) %all-to-all-start.5) | async-done | bytes 2097184 | tf_op jit(solution)/shard_map/all_to_all | solution.py:215
  (218 shorter events, 279.3 us)
Async XLA Ops:
  6.5 488.0 %copy-start = (bf16[1,512,2048]{2,1,0:T(8,128)(2,1)S(1)}, bf16[1,512,2048]{2,1,0:T(8,128)(2,1)}, u32[]{:S(2)}) copy-start(bf16[1,512,2048]{2,1,0:T(8,128)(2,1)} %param.37) | copy-start | bytes 6291460
  6.5 21.6 %copy-start.7 = (s32[128,2]{0,1:T(2,128)S(1)}, s32[128,2]{0,1:T(2,128)}, u32[]{:S(2)}) copy-start(s32[128,2]{0,1:T(2,128)} %param.38) | copy-start | bytes 3076
  6.5 23.2 %copy-start.4 = (bf16[256,512]{1,0:T(8,128)(2,1)S(1)}, bf16[256,512]{1,0:T(8,128)(2,1)}, u32[]{:S(2)}) copy-start(bf16[256,512]{1,0:T(8,128)(2,1)} %param.23) | copy-start | bytes 786436
  6.5 89.5 %all-gather.4.cloned.1.call-start = ((), (), s32[]{:S(2)}) async-start(), calls=%async_computation.6 | async-start | bytes 2129920 | tf_op jit(solution)/shard_map/all_gather | solution.py:159
  9.0 20.8 %copy-start.12 = (f32[64]{0:T(128)S(1)}, f32[64]{0:T(128)}, u32[]{:S(2)}) copy-start(f32[64]{0:T(128)} %param.29) | copy-start | bytes 772
  9.8 313.2 %all-gather.6.cloned.1.call-start = ((), (), s32[]{:S(2)}) async-start(), calls=%async_computation.7 | async-start | bytes 4259840 | tf_op jit(solution)/shard_map/all_gather | solution.py:163
  12.3 18.8 %copy-start.13 = (f32[128]{0:T(128)S(1)}, f32[128]{0:T(128)}, u32[]{:S(2)}) copy-start(f32[128]{0:T(128)} %param.31) | copy-start | bytes 1540
  15.6 41.9 %all-to-all-start = ((bf16[64,256,64]{1,2,0:T(8,128)(2,1)}), bf16[64,256,64]{1,2,0:T(8,128)(2,1)}, u32[]{:S(2)}, u32[]{:S(2)}) async-start(bf16[64,256,64]{1,2,0:T(8,128)(2,1)} %stack.36), calls=%async_computation | async-start | bytes 4194304 | tf_op jit(solution)/shard_map/all_to_all | solution.py:161
  27.4 302.0 %all-gather.8.cloned.1.call-start = ((), (), s32[]{:S(2)}) async-start(), calls=%async_computation.8 | async-start | bytes 4259840 | tf_op jit(solution)/shard_map/all_gather | solution.py:164
  34.9 6.8 %copy-start.5 = (s32[256]{0:T(256)}, s32[256]{0:T(256)S(1)}, u32[]{:S(2)}) copy-start(s32[256]{0:T(256)S(1)} %fusion.78) | copy-start | bytes 3076
  335.4 5.9 %copy-start.1 = (f32[2048,256,4]{1,0,2:T(8,128)S(1)}, f32[2048,256,4]{1,0,2:T(8,128)}, u32[]{:S(2)}) copy-start(f32[2048,256,4]{1,0,2:T(8,128)} %get-tuple-element.357) | copy-start | bytes 25165828 | tf_op jit(solution)/shard_map/while
  348.3 5.9 %copy-start.1 = (f32[2048,256,4]{1,0,2:T(8,128)S(1)}, f32[2048,256,4]{1,0,2:T(8,128)}, u32[]{:S(2)}) copy-start(f32[2048,256,4]{1,0,2:T(8,128)} %get-tuple-element.357) | copy-start | bytes 25165828 | tf_op jit(solution)/shard_map/while
  361.2 5.9 %copy-start.1 = (f32[2048,256,4]{1,0,2:T(8,128)S(1)}, f32[2048,256,4]{1,0,2:T(8,128)}, u32[]{:S(2)}) copy-start(f32[2048,256,4]{1,0,2:T(8,128)} %get-tuple-element.357) | copy-start | bytes 25165828 | tf_op jit(solution)/shard_map/while
  374.0 5.9 %copy-start.1 = (f32[2048,256,4]{1,0,2:T(8,128)S(1)}, f32[2048,256,4]{1,0,2:T(8,128)}, u32[]{:S(2)}) copy-start(f32[2048,256,4]{1,0,2:T(8,128)} %get-tuple-element.357) | copy-start | bytes 25165828 | tf_op jit(solution)/shard_map/while
  386.9 5.9 %copy-start.1 = (f32[2048,256,4]{1,0,2:T(8,128)S(1)}, f32[2048,256,4]{1,0,2:T(8,128)}, u32[]{:S(2)}) copy-start(f32[2048,256,4]{1,0,2:T(8,128)} %get-tuple-element.357) | copy-start | bytes 25165828 | tf_op jit(solution)/shard_map/while
  399.7 5.9 %copy-start.1 = (f32[2048,256,4]{1,0,2:T(8,128)S(1)}, f32[2048,256,4]{1,0,2:T(8,128)}, u32[]{:S(2)}) copy-start(f32[2048,256,4]{1,0,2:T(8,128)} %get-tuple-element.357) | copy-start | bytes 25165828 | tf_op jit(solution)/shard_map/while
  412.6 5.9 %copy-start.1 = (f32[2048,256,4]{1,0,2:T(8,128)S(1)}, f32[2048,256,4]{1,0,2:T(8,128)}, u32[]{:S(2)}) copy-start(f32[2048,256,4]{1,0,2:T(8,128)} %get-tuple-element.357) | copy-start | bytes 25165828 | tf_op jit(solution)/shard_map/while
  425.5 5.9 %copy-start.1 = (f32[2048,256,4]{1,0,2:T(8,128)S(1)}, f32[2048,256,4]{1,0,2:T(8,128)}, u32[]{:S(2)}) copy-start(f32[2048,256,4]{1,0,2:T(8,128)} %get-tuple-element.357) | copy-start | bytes 25165828 | tf_op jit(solution)/shard_map/while
  481.5 9.4 %copy-start.14 = (bf16[1,2048,512]{2,1,0:T(8,128)(2,1)S(1)}, bf16[1,2048,512]{2,1,0:T(8,128)(2,1)}, u32[]{:S(2)}) copy-start(bf16[1,2048,512]{2,1,0:T(8,128)(2,1)} %param.36) | copy-start | bytes 6291460
  516.5 11.3 %copy-start.8 = (s32[128,2]{0,1:T(2,128)S(1)}, s32[128,2]{0,1:T(2,128)}, u32[]{:S(2)}) copy-start(s32[128,2]{0,1:T(2,128)} %param.38) | copy-start | bytes 3076
  516.5 11.5 %copy-start.10 = (pred[128,2]{0,1:T(4,128)(4,1)S(1)}, pred[128,2]{0,1:T(4,128)(4,1)}, u32[]{:S(2)}) copy-start(pred[128,2]{0,1:T(4,128)(4,1)} %get-tuple-element.221) | copy-start | bytes 772
  516.5 11.7 %copy-start.11 = (f32[128,2]{0,1:T(2,128)S(1)}, f32[128,2]{0,1:T(2,128)}, u32[]{:S(2)}) copy-start(f32[128,2]{0,1:T(2,128)} %param.39) | copy-start | bytes 3076
  516.5 11.8 %copy-start.6 = (s32[256]{0:T(256)S(1)}, s32[256]{0:T(256)}, u32[]{:S(2)}) copy-start(s32[256]{0:T(256)} %copy-done.5) | copy-start | bytes 3076
  521.6 36.4 %all-to-all-start.5 = ((bf16[64,8,2048]{2,1,0:T(8,128)(2,1)}), bf16[64,8,2048]{2,1,0:T(8,128)(2,1)}, u32[]{:S(2)}, u32[]{:S(2)}) async-start(bf16[64,8,2048]{2,1,0:T(8,128)(2,1)} %reduce_sum.131), calls=%async_computation.5 | async-start | bytes 4194304 | tf_op jit(solution)/shard_map/all_to_all | solution.py:215
  (3 other events, 12.1 us)
Sparse Core Ops, SparseCore 0:
  10.0 85.9 all-gather.3
  98.8 73.9 all-gather.5
  175.7 69.3 all-gather.7
